TPU v7x, 32 devices: a whole 2x2x4 slice. The times are simulated.
32 devices in a mesh: grp: 2 (over y), fs: 4 (over z), tp: 4 (over x, core).
Axes of the slice: x: 2, y: 2, z: 4, core: 2. Of those that a mesh axis runs over, the one named last changes fastest.
Arguments:
- tokens: bfloat16 [6144, 2048], P(('grp', 'fs')), parts along dimension 0, may hold values from -6 to 6
- up_weight: bfloat16 [2048, 8192], P('fs', 'tp'), may hold values from -0.125 to 0.125
- down_weight: bfloat16 [8192, 2048], P('tp', 'fs'), may hold values from -0.0625 to 0.0625
- norm_gain: float32 [2048], replicated, may hold values from 0.1 to 1.9
- norm_shift: float32 [2048], replicated, may hold values from -3 to 3
Outputs:
- mixed: bfloat16 [6144, 2048], P(('grp', 'fs')), parts along dimension 0
There are 2 independent parts, one for each index of `grp`. A program takes and returns all parts, laid end to end along the dimension named above; an argument that names none is the same for every part. Nothing has to cross between parts.
All inputs are finite; a program needn't handle non-finite values.
Results may differ from a plain program's by a relative error of at most 0.014.
Values may be sent and summed in bfloat16 or wider, within the bound.
A program may use at most 64 MiB of HBM per device.

v0:
```python
import jax
import jax.numpy as jnp
from jax import lax
from jax.sharding import PartitionSpec as P

RESIDUAL_SCALE = 2.0**0.25
NORM_EPS = 1e-05


def layer_normed(residual, summed, norm_gain, norm_shift):
    pre_norm = RESIDUAL_SCALE * residual.astype(jnp.float32) + summed
    centre = jnp.mean(pre_norm, axis=-1, keepdims=True)
    centered = pre_norm - centre
    variance = jnp.mean(centered * centered, axis=-1, keepdims=True)
    return (centered * lax.rsqrt(variance + NORM_EPS) * norm_gain + norm_shift).astype(jnp.bfloat16)


def shards(tokens, up_weight, down_weight, norm_gain, norm_shift):
    upward = jnp.dot(
        tokens,
        lax.all_gather(up_weight, "fs", axis=0, tiled=True),
        preferred_element_type=jnp.float32,
    )
    down_full = lax.all_gather(down_weight, "fs", axis=1, tiled=True)
    hidden = jnp.square(jax.nn.relu(upward)).astype(jnp.bfloat16)
    share = tokens.shape[0] // lax.axis_size("tp")
    summed = lax.psum_scatter(
        jnp.dot(hidden, down_full, preferred_element_type=jnp.float32).astype(jnp.bfloat16),
        "tp",
        scatter_dimension=0,
        tiled=True,
    ).astype(jnp.float32)
    own_start = lax.axis_index("tp") * share
    own_tokens = lax.dynamic_slice_in_dim(tokens, own_start, share, 0)
    normed = layer_normed(own_tokens, summed, norm_gain, norm_shift)
    return lax.all_gather(normed, "tp", axis=0, tiled=True)


def solution(mesh):
    placed = (P(("grp", "fs"), None), P("fs", "tp"), P("tp", "fs"), P(), P())
    return jax.shard_map(
        shards, mesh=mesh, in_specs=placed, out_specs=P(("grp", "fs"), None), check_vma=False
    )
```

profile of v0, /device:TPU:1, one launch (start us, length us, event | category | flops | bytes accessed | tf_op | source)
XLA Modules:
  0.0 402.2 jit_solution(14046685828102496257)
XLA Ops:
  6.5 0.0 copy-start.1
  6.5 0.0 all-gather.4.cloned.1.call-start
  6.5 0.7 all-gather.4.cloned.1.call-update
  7.3 0.0 all-gather.6.cloned.1.call-start
  7.3 0.7 all-gather.6.cloned.1.call-update
  8.0 0.0 reduce-scatter.2.cloned.1.call-start
  8.1 152.7 %all-gather.4.cloned.1.call-done = bf16[2048,2048]{1,0:T(8,128)(2,1)} async-done(((bf16[512,2048]{1,0:T(8,128)(2,1)}), bf16[2048,2048]{1,0:T(8,128)(2,1)}) %all-gather.4.cloned.1.call-update) | async-done | bytes 8388624 | tf_op jit(solution)/shard_map/all_gather | solution.py:21
  160.8 0.0 copy-done.1
  160.8 10.2 %multiply_convert_fusion = bf16[768,2048]{1,0:T(8,128)(2,1)} fusion(bf16[768,2048]{1,0:T(8,128)(2,1)S(1)} %copy-done.1, bf16[2048,2048]{1,0:T(8,128)(2,1)} %all-gather.4.cloned.1.call-done), kind=kOutput, calls=%fused_computation | convolution fusion | flops 6447169536 | bytes 14680064 | tf_op jit(solution)/shard_map/dot_general | solution.py:19
  171.0 139.2 %all-gather.6.cloned.1.call-done = bf16[2048,2048]{1,0:T(8,128)(2,1)} async-done(((bf16[2048,512]{1,0:T(8,128)(2,1)}), bf16[2048,2048]{1,0:T(8,128)(2,1)}) %all-gather.6.cloned.1.call-update) | async-done | bytes 8388624 | tf_op jit(solution)/shard_map/all_gather | solution.py:24
  310.2 11.9 %convolution_convert_fusion = bf16[768,2048]{1,0:T(8,128)(2,1)} fusion(bf16[768,2048]{1,0:T(8,128)(2,1)} %multiply_convert_fusion, bf16[2048,2048]{1,0:T(8,128)(2,1)} %all-gather.6.cloned.1.call-done), kind=kOutput, calls=%fused_computation.1 | convolution fusion | flops 6444023808 | bytes 14680064 | tf_op jit(solution)/shard_map/dot_general | solution.py:28
  322.0 0.0 copy-start.2
  322.0 0.0 reduce-scatter.2.cloned.1.call-update
  322.1 0.0 all-gather.8.cloned.1.call-start
  322.1 35.8 %reduce-scatter.2.cloned.1.call-done = bf16[192,2048]{1,0:T(8,128)(2,1)} async-done(((bf16[768,2048]{1,0:T(8,128)(2,1)}), bf16[192,2048]{1,0:T(8,128)(2,1)}) %reduce-scatter.2.cloned.1.call-update) | async-done | bytes 786448 | tf_op jit(solution)/shard_map/reduce_scatter | solution.py:27
  358.0 1.5 fusion
  359.5 1.6 multiply_reduce_fusion
  361.1 0.0 copy-done.2
  361.1 0.0 copy-done.3
  361.1 0.0 copy-done
  361.1 1.4 add_convert_fusion
  362.5 0.0 all-gather.8.cloned.1.call-update
  362.5 29.2 %all-gather.8.cloned.1.call-done = bf16[768,2048]{1,0:T(8,128)(2,1)} async-done(((bf16[192,2048]{1,0:T(8,128)(2,1)}), bf16[768,2048]{1,0:T(8,128)(2,1)}) %all-gather.8.cloned.1.call-update) | async-done | bytes 3145744 | tf_op jit(solution)/shard_map/all_gather | solution.py:36
  391.7 4.0 copy.7
  (4 shorter events, 0.0 us)
Async XLA Ops:
  6.5 154.2 %copy-start.1 = (bf16[768,2048]{1,0:T(8,128)(2,1)S(1)}, bf16[768,2048]{1,0:T(8,128)(2,1)}, u32[]{:S(2)}) copy-start(bf16[768,2048]{1,0:T(8,128)(2,1)} %param.5) | copy-start | bytes 9437188
  6.5 154.2 %all-gather.4.cloned.1.call-start = ((), (), s32[]{:S(2)}) async-start(), calls=%async_computation.1 | async-start | bytes 10485760 | tf_op jit(solution)/shard_map/all_gather | solution.py:21
  7.3 302.9 %all-gather.6.cloned.1.call-start = ((), (), s32[]{:S(2)}) async-start(), calls=%async_computation.2 | async-start | bytes 10485760 | tf_op jit(solution)/shard_map/all_gather | solution.py:24
  8.0 350.0 %reduce-scatter.2.cloned.1.call-start = ((), (), s32[]{:S(2)}) async-start(), calls=%async_computation.3 | async-start | bytes 3932160 | tf_op jit(solution)/shard_map/reduce_scatter | solution.py:27
  322.0 39.1 %copy-start.2 = (f32[2048]{0:T(1024)S(1)}, f32[2048]{0:T(1024)}, u32[]{:S(2)}) copy-start(f32[2048]{0:T(1024)} %param.9) | copy-start | bytes 24580
  322.0 39.1 %copy-start.3 = (f32[2048]{0:T(1024)S(1)}, f32[2048]{0:T(1024)}, u32[]{:S(2)}) copy-start(f32[2048]{0:T(1024)} %param.8) | copy-start | bytes 24580
  322.1 69.7 %all-gather.8.cloned.1.call-start = ((), (), s32[]{:S(2)}) async-start(), calls=%async_computation.4 | async-start | bytes 3932160 | tf_op jit(solution)/shard_map/all_gather | solution.py:36
  358.0 3.2 copy-start
Sparse Core Ops, SparseCore 0:
  8.9 151.8 all-gather.3
  162.3 147.7 all-gather.5
  322.2 35.7 reduce-scatter.1
  362.6 29.0 all-gather.7
where the time goes:
time: 403 us; the launch traced here: 402 us
  waiting for transfers between devices  358 us (89%)
  matrix products  22 us (5%)
  between operations  13.2 us (3%)
  other arithmetic  4.49 us (1%)
    all_gather x1, waiting for transfers between devices, shards(): lax.all_gather(up_weight, 'fs', axis=0, tiled=True)  153 us
    all_gather x1, waiting for transfers between devices, shards(): down_full = lax.all_gather(down_weight, 'fs', axis=1, tiled=True)  139 us
    reduce_scatter x1, waiting for transfers between devices, shards(): lax.psum_scatter(jnp.dot(hidden, down_full, preferred_element_type=jnp.fl...  35.8 us
    all_gather x1, waiting for transfers between devices, shards(): return lax.all_gather(normed, 'tp', axis=0, tiled=True)  29.2 us
    dot_general x1, matrix products, shards(): jnp.dot(hidden, down_full, preferred_element_type=jnp.float32)  11.9 us
    dot_general x1, matrix products, shards(): jnp.dot(tokens, lax.all_gather(up_weight, 'fs', axis=0, tiled=True), pref...  10.2 us
  transfers between devices with their start and end apart: 4, of which 4 were waited for; matrix products, arithmetic and copies ran while one was open for 3% of the time, Pallas kernels for 0%

commit v1 on v0

--- a/solution.py
+++ b/solution.py
@@ -1,10 +1,16 @@
+import functools
+
 import jax
 import jax.numpy as jnp
 from jax import lax
+from jax.experimental import pallas as pl
+from jax.experimental.pallas import tpu as pltpu
 from jax.sharding import PartitionSpec as P
 
+MESH = pl.DeviceIdType.MESH
 RESIDUAL_SCALE = 2.0**0.25
 NORM_EPS = 1e-05
+SUBS = 4
 
 
 def layer_normed(residual, summed, norm_gain, norm_shift):
@@ -15,7 +21,7 @@
     return (centered * lax.rsqrt(variance + NORM_EPS) * norm_gain + norm_shift).astype(jnp.bfloat16)
 
 
-def shards(tokens, up_weight, down_weight, norm_gain, norm_shift):
+def general(tokens, up_weight, down_weight, norm_gain, norm_shift):
     upward = jnp.dot(
         tokens,
         lax.all_gather(up_weight, "fs", axis=0, tiled=True),
@@ -36,8 +42,339 @@
     return lax.all_gather(normed, "tp", axis=0, tiled=True)
 
 
+def arrival_order(n):
+    table = []
+    for f in range(n):
+        inward = 1 if f < n // 2 else -1
+        order = []
+        for d in range(1, n):
+            for s in (f + inward * d, f - inward * d):
+                if 0 <= s < n:
+                    order.append(s)
+        table.append(order)
+    return table
+
+
+def kernel(
+    n,
+    tok_hbm, up_hbm, down_hbm, gain_ref, shift_ref,
+    out_ref,
+    tok, U, Dn, acc, hid, part, half_in, pair, pair_in, summed,
+    loc_sem, z_send, z_recv, y_send, y_recv, a_send, a_recv, b_send, b_recv, c_send, c_recv,
+):
+    g, f, t = lax.axis_index("grp"), lax.axis_index("fs"), lax.axis_index("tp")
+    core = lax.rem(t, 2)
+    other_g = 1 - g
+    mate = t + 1 - 2 * core
+    across = lax.rem(t + 2, 4)
+    rows, width = tok.shape
+    depth = U.shape[1]
+    hd = depth // 2
+    ff = U.shape[2]
+    hw = Dn.shape[3]
+    half_rows = rows // 2
+
+    table = arrival_order(n)
+
+    def taken(k):
+        s = jnp.int32(table[0][k])
+        for i in range(1, n):
+            s = jnp.where(f == i, table[i][k], s)
+        return s
+
+    order = [taken(k) for k in range(n - 1)]
+
+    def own_up(h, sem):
+        r = pl.ds(pl.multiple_of(h * hd, hd), hd)
+        return pltpu.make_async_copy(up_hbm.at[r, :], U.at[f, r, :], loc_sem.at[sem])
+
+    def own_down(h, sem):
+        c = pl.ds(pl.multiple_of(h * hw, hw), hw)
+        return pltpu.make_async_copy(down_hbm.at[:, c], Dn.at[f, h], loc_sem.at[sem])
+
+    local = [
+        own_up(g, 0),
+        pltpu.make_async_copy(tok_hbm, tok, loc_sem.at[1]),
+        own_up(other_g, 2),
+        own_down(g, 3),
+        own_down(other_g, 4),
+    ]
+    for c in local:
+        c.start()
+
+    barrier = pltpu.get_barrier_semaphore()
+    for dev in ({"grp": other_g}, {"tp": mate}, {"tp": across}):
+        pl.semaphore_signal(barrier, inc=1, device_id=dev, device_id_type=MESH)
+
+    @pl.when(f > 0)
+    def _():
+        pl.semaphore_signal(barrier, inc=1, device_id={"fs": f - 1}, device_id_type=MESH)
+
+    @pl.when(f < n - 1)
+    def _():
+        pl.semaphore_signal(barrier, inc=1, device_id={"fs": f + 1}, device_id_type=MESH)
+
+    pl.semaphore_wait(barrier, 3 + (f > 0).astype(jnp.int32) + (f < n - 1).astype(jnp.int32))
+
+    def piece(array, s, h, sub):
+        if array == 0:
+            m = hd // SUBS
+            return U.at[s, pl.ds(pl.multiple_of(h * hd + sub * m, m), m), :]
+        m = ff // SUBS
+        return Dn.at[s, h, pl.ds(pl.multiple_of(sub * m, m), m), :]
+
+    def z_copy(array, s, sub, way):
+        ref = piece(array, s, g, sub)
+        return pltpu.make_async_remote_copy(
+            src_ref=ref, dst_ref=ref,
+            send_sem=z_send.at[array, s, sub, way], recv_sem=z_recv.at[array, s, sub],
+            device_id={"fs": f + (2 * way - 1)}, device_id_type=MESH,
+        )
+
+    def y_copy(array, s, h, sub):
+        ref = piece(array, s, h, sub)
+        return pltpu.make_async_remote_copy(
+            src_ref=ref, dst_ref=ref,
+            send_sem=y_send.at[array, s, sub], recv_sem=y_recv.at[array, s, sub],
+            device_id={"grp": other_g}, device_id_type=MESH,
+        )
+
+    def own_sends(array, sub, act):
+        @pl.when(f > 0)
+        def _():
+            act(z_copy(array, f, sub, 0))
+
+        @pl.when(f < n - 1)
+        def _():
+            act(z_copy(array, f, sub, 1))
+
+    def passes(array, s, sub, act):
+        @pl.when((s > f) & (f > 0))
+        def _():
+            act(z_copy(array, s, sub, 0))
+
+        @pl.when((s < f) & (f < n - 1))
+        def _():
+            act(z_copy(array, s, sub, 1))
+
+    start = lambda copy: copy.start()
+    sent = lambda copy: copy.wait_send()
+
+    def take(array, k, after=None):
+        s = order[k]
+
+        def body(sub, carry):
+            z_copy(array, s, sub, 0).wait_recv()
+            passes(array, s, sub, start)
+            y_copy(array, s, g, sub).start()
+            if after is not None:
+                after(sub)
+            return carry
+
+        lax.fori_loop(0, SUBS, body, 0)
+
+    def take_y(array, k):
+        s = order[k]
+
+        def body(sub, carry):
+            y_copy(array, s, other_g, sub).wait_recv()
+            return carry
+
+        lax.fori_loop(0, SUBS, body, 0)
+
+    def up_dot(s, h, first=False):
+        r = pl.ds(pl.multiple_of(h * hd, hd), hd)
+        kc = pl.ds(pl.multiple_of(s * depth + h * hd, hd), hd)
+        tile = ff // 4
+
+        def body(j, carry):
+            js = pl.ds(pl.multiple_of(j * tile, tile), tile)
+            got = jnp.dot(tok[:, kc], U[s, r, js], preferred_element_type=jnp.float32)
+            if first:
+                acc[:, js] = got
+            else:
+                acc[:, js] += got
+            return carry
+
+        lax.fori_loop(0, 4, body, 0)
+
+    own_half = pl.ds(pl.multiple_of(core * half_rows, half_rows), half_rows)
+    mate_half = pl.ds(pl.multiple_of((1 - core) * half_rows, half_rows), half_rows)
+
+    def a_copy(q):
+        return pltpu.make_async_remote_copy(
+            src_ref=part.at[q, mate_half, :], dst_ref=half_in.at[q],
+            send_sem=a_send.at[q], recv_sem=a_recv.at[q],
+            device_id={"tp": mate}, device_id_type=MESH,
+        )
+
+    def b_copy(q):
+        return pltpu.make_async_remote_copy(
+            src_ref=pair.at[q], dst_ref=pair_in.at[q],
+            send_sem=b_send.at[q], recv_sem=b_recv.at[q],
+            device_id={"tp": across}, device_id_type=MESH,
+        )
+
+    def c_copy(q):
+        ref = summed.at[q, own_half, :]
+        return pltpu.make_async_remote_copy(
+            src_ref=ref, dst_ref=ref,
+            send_sem=c_send.at[q], recv_sem=c_recv.at[q],
+            device_id={"tp": mate}, device_id_type=MESH,
+        )
+
+    def down_dot(s, h):
+        q = s * 2 + h
+        tile = rows // 3
+
+        def body(i, carry):
+            r = pl.ds(pl.multiple_of(i * tile, tile), tile)
+            part[q, r, :] = jnp.dot(
+                hid[r, :], Dn[s, h], preferred_element_type=jnp.float32
+            ).astype(jnp.bfloat16)
+            return carry
+
+        lax.fori_loop(0, 3, body, 0)
+        a_copy(q).start()
+
+    def chip_sum(q):
+        a_copy(q).wait_recv()
+        pair[q] = (
+            part[q, own_half, :].astype(jnp.float32) + half_in[q].astype(jnp.float32)
+        ).astype(jnp.bfloat16)
+        b_copy(q).start()
+
+    def full_sum(q):
+        b_copy(q).wait_recv()
+        summed[q, own_half, :] = pair[q].astype(jnp.float32) + pair_in[q].astype(jnp.float32)
+        c_copy(q).start()
+
+    local[0].wait()
+    lax.fori_loop(0, SUBS, lambda sub, c: (own_sends(0, sub, start), c)[1], 0)
+    for c in local[1:]:
+        c.wait()
+    up_dot(f, 0, first=True)
+    up_dot(f, 1)
+    for k in range(n - 1):
+        after = None
+        if k == 1:
+            after = lambda sub: own_sends(1, sub, start)
+        take(0, k, after)
+        up_dot(order[k], g)
+        if k > 0:
+            take_y(0, k - 1)
+            up_dot(order[k - 1], other_g)
+    take(1, 0)
+    take_y(0, n - 2)
+    up_dot(order[n - 2], other_g)
+
+    def activate(i, carry):
+        m = rows // 12
+        r = pl.ds(pl.multiple_of(i * m, m), m)
+        hid[r, :] = jnp.square(jnp.maximum(acc[r, :], 0.0)).astype(jnp.bfloat16)
+        return carry
+
+    lax.fori_loop(0, 12, activate, 0)
+
+    done = []
+
+    def block(s, h):
+        down_dot(s, h)
+        done.append(s * 2 + h)
+        if len(done) > 1:
+            chip_sum(done[-2])
+        if len(done) > 2:
+            full_sum(done[-3])
+
+    block(f, g)
+    block(f, other_g)
+    block(order[0], g)
+    for k in range(1, n - 1):
+        take(1, k)
+        block(order[k], g)
+        take_y(1, k - 1)
+        block(order[k - 1], other_g)
+    take_y(1, n - 2)
+    block(order[n - 2], other_g)
+    chip_sum(done[-1])
+    full_sum(done[-2])
+    full_sum(done[-1])
+    for q in range(2 * n):
+        pltpu.make_async_remote_copy(
+            src_ref=summed.at[q, mate_half, :], dst_ref=summed.at[q, mate_half, :],
+            send_sem=c_send.at[q], recv_sem=c_recv.at[q],
+            device_id={"tp": mate}, device_id_type=MESH,
+        ).wait_recv()
+
+    def norm(i, carry):
+        m = 16
+        r = pl.ds(pl.multiple_of(i * m, m), m)
+        total = jnp.concatenate([summed[q, r, :] for q in range(2 * n)], axis=-1)
+        out_ref[r, :] = layer_normed(tok[r, :], total, gain_ref[...], shift_ref[...])
+        return carry
+
+    lax.fori_loop(0, rows // 16, norm, 0)
+
+    def drain(sub, carry):
+        for array in range(2):
+            own_sends(array, sub, sent)
+            for k in range(n - 1):
+                passes(array, order[k], sub, sent)
+                y_copy(array, order[k], g, sub).wait_send()
+        return carry
+
+    lax.fori_loop(0, SUBS, drain, 0)
+    for q in range(2 * n):
+        a_copy(q).wait_send()
+        b_copy(q).wait_send()
+        c_copy(q).wait_send()
+
+
+def direct(n, tokens, up_weight, down_weight, norm_gain, norm_shift):
+    rows, width = tokens.shape
+    depth, ff = up_weight.shape
+    hw = down_weight.shape[1] // 2
+    blocks = 2 * n
+    bf16, f32 = jnp.bfloat16, jnp.float32
+    dma = pltpu.SemaphoreType.DMA
+    anywhere = pl.BlockSpec(memory_space=pl.ANY)
+    vmem = pl.BlockSpec(memory_space=pltpu.VMEM)
+    return pl.pallas_call(
+        functools.partial(kernel, n),
+        out_shape=jax.ShapeDtypeStruct((rows, width), bf16),
+        in_specs=[anywhere, anywhere, anywhere, vmem, vmem],
+        out_specs=vmem,
+        scratch_shapes=[
+            pltpu.VMEM((rows, width), bf16),
+            pltpu.VMEM((n, depth, ff), bf16),
+            pltpu.VMEM((n, 2, ff, hw), bf16),
+            pltpu.VMEM((rows, ff), f32),
+            pltpu.VMEM((rows, ff), bf16),
+            pltpu.VMEM((blocks, rows, hw), bf16),
+            pltpu.VMEM((blocks, rows // 2, hw), bf16),
+            pltpu.VMEM((blocks, rows // 2, hw), bf16),
+            pltpu.VMEM((blocks, rows // 2, hw), bf16),
+            pltpu.VMEM((blocks, rows, hw), f32),
+            dma((5,)),
+            dma((2, n, SUBS, 2)),
+            dma((2, n, SUBS)),
+            dma((2, n, SUBS)),
+            dma((2, n, SUBS)),
+            dma((blocks,)), dma((blocks,)),
+            dma((blocks,)), dma((blocks,)),
+            dma((blocks,)), dma((blocks,)),
+        ],
+        compiler_params=pltpu.CompilerParams(
+            collective_id=0, has_side_effects=True, vmem_limit_bytes=60 * 1024 * 1024
+        ),
+    )(tokens, up_weight, down_weight, norm_gain[None, :], norm_shift[None, :])
+
+
 def solution(mesh):
     placed = (P(("grp", "fs"), None), P("fs", "tp"), P("tp", "fs"), P(), P())
+    n = mesh.shape["fs"]
+    fits = mesh.shape["grp"] == 2 and mesh.shape["tp"] == 4 and n == 4
     return jax.shard_map(
-        shards, mesh=mesh, in_specs=placed, out_specs=P(("grp", "fs"), None), check_vma=False
+        functools.partial(direct, n) if fits else general,
+        mesh=mesh, in_specs=placed, out_specs=P(("grp", "fs"), None), check_vma=False,
     )

time: 403 us -> 201 us (0.50)
  waiting for transfers between devices: 358 us -> 0 us
  Pallas kernels: 0 us -> 196 us
  matrix products: 22 us -> 0 us
  between operations: 13.2 us -> 0.01 us
  other arithmetic: 4.49 us -> 0 us
    all_gather x3 -> x0, waiting for transfers between devices: 321 us -> none  [the longest x1 153 us: shards(): lax.all_gather(up_weight, 'fs', axis=0, tiled=True)]
    pallas_call x0 -> x1, Pallas kernels: none -> 196 us  [direct(): pl.pallas_call(functools.partial(kernel, n), out_shape=jax.ShapeDtypeStru...]
    reduce_scatter x1 -> x0, waiting for transfers between devices: 35.8 us -> none  [shards(): lax.psum_scatter(jnp.dot(hidden, down_full, preferred_element_type=jnp.fl...]
    dot_general x2 -> x0, matrix products: 22 us -> none  [the longest x1 11.9 us: shards(): jnp.dot(hidden, down_full, preferred_element_type=jnp.float32)]
  transfers between devices with their start and end apart: 4 -> 0, of which waited for: 4 -> 0; matrix products, arithmetic and copies ran while one was open for 3% -> 0% of each run, Pallas kernels for 0% -> 0%
where the time goes in v1:
time: 201 us; the launch traced here: 200 us
  Pallas kernels  196 us (98%)
  local copies, waits for them, and re-layouts  3.97 us (2%)
    pallas_call x1, Pallas kernels, direct(): pl.pallas_call(functools.partial(kernel, n), out_shape=jax.ShapeDtypeStru...  196 us

profile of v1, /device:TPU:1, one launch (start us, length us, event | category | flops | bytes accessed | tf_op | source)
XLA Modules:
  0.0 200.4 jit_solution(3126233206604647098)
XLA Ops:
  0.0 196.4 %shard_map.55 = bf16[768,2048]{1,0:T(8,128)(2,1)} custom-call(bf16[768,2048]{1,0:T(8,128)(2,1)} %tok_hbm.1, bf16[512,2048]{1,0:T(8,128)(2,1)} %up_hbm.1, bf16[2048,512]{1,0:T(8,128)(2,1)} %down_hbm.1, f32[1,2048]{1,0:T(1,128)} %bitcast.2, f32[1,2048]{1,0:T(1,128)} %bitcast.3), custom_call_target="tpu_custom_call" | custom-call | tf_op jit(solution)/shard_map/pallas_call | solution.py:342
  196.4 4.0 %copy.7 = bf16[768,2048]{1,0:T(8,128)(2,1)} copy(bf16[768,2048]{1,0:T(8,128)(2,1)} %shard_map.55) | data formatting | bytes 6291456

commit v2 on v0

--- a/solution.py
+++ b/solution.py
@@ -1,10 +1,16 @@
+import functools
+
 import jax
 import jax.numpy as jnp
 from jax import lax
+from jax.experimental import pallas as pl
+from jax.experimental.pallas import tpu as pltpu
 from jax.sharding import PartitionSpec as P
 
+MESH = pl.DeviceIdType.MESH
 RESIDUAL_SCALE = 2.0**0.25
 NORM_EPS = 1e-05
+SUBS = 4
 
 
 def layer_normed(residual, summed, norm_gain, norm_shift):
@@ -15,7 +21,7 @@
     return (centered * lax.rsqrt(variance + NORM_EPS) * norm_gain + norm_shift).astype(jnp.bfloat16)
 
 
-def shards(tokens, up_weight, down_weight, norm_gain, norm_shift):
+def general(tokens, up_weight, down_weight, norm_gain, norm_shift):
     upward = jnp.dot(
         tokens,
         lax.all_gather(up_weight, "fs", axis=0, tiled=True),
@@ -36,8 +42,388 @@
     return lax.all_gather(normed, "tp", axis=0, tiled=True)
 
 
+def kernel(
+    n,
+    tok_hbm, up_hbm, down_hbm, gain_ref, shift_ref,
+    out_ref,
+    tok, U, Dn, acc, hid, part, half_in, pair, pair_in, summed, quarter,
+    loc_sem, z_send, z_recv, y_send, y_recv, t_send, t_recv, g_send, g_recv,
+    a_send, a_recv, b_send, b_recv, c_send, c_recv, e_send, e_recv, h_send, h_recv,
+):
+    g, f, t = lax.axis_index("grp"), lax.axis_index("fs"), lax.axis_index("tp")
+    core, chip = lax.rem(t, 2), t // 2
+    other_g = 1 - g
+    mate = t + 1 - 2 * core
+    across = lax.rem(t + 2, 4)
+    pal = f + 1 - 2 * lax.rem(f, 2)
+    inner = (f > 0) & (f < n - 1)
+    fi, fo = jnp.where(inner, f, pal), jnp.where(inner, pal, f)
+    ri, ro = n - 1 - fi, n - 1 - fo
+    rows, width = out_ref.shape
+    depth, ff, hw = U.shape[1], U.shape[2], Dn.shape[3]
+    hd = depth // 2
+    hr, qr = rows // 2, rows // 4
+    place = core * 2 + chip
+    blocks = 2 * n
+
+    def own_up(h, sem):
+        r = pl.ds(pl.multiple_of(h * hd, hd), hd)
+        return pltpu.make_async_copy(up_hbm.at[r, :], U.at[f, r, :], loc_sem.at[sem])
+
+    def own_down(h, sem):
+        c = pl.ds(pl.multiple_of(h * hw, hw), hw)
+        return pltpu.make_async_copy(down_hbm.at[:, c], Dn.at[f, h], loc_sem.at[sem])
+
+    local = [
+        own_up(g, 0),
+        pltpu.make_async_copy(tok_hbm, tok.at[pl.ds(0, rows), :], loc_sem.at[1]),
+        own_up(other_g, 2),
+        own_down(g, 3),
+        own_down(other_g, 4),
+    ]
+    for c in local:
+        c.start()
+
+    barrier = pltpu.get_barrier_semaphore()
+    peers = [lax.rem(t + d, 4) for d in (1, 2, 3)]
+    for dev in [{"grp": other_g}, {"fs": pal}] + [{"tp": p} for p in peers]:
+        pl.semaphore_signal(barrier, inc=1, device_id=dev, device_id_type=MESH)
+
+    @pl.when(inner)
+    def _():
+        pl.semaphore_signal(barrier, inc=1, device_id={"fs": n - 1 - f}, device_id_type=MESH)
+
+    pl.semaphore_wait(barrier, 5 + inner.astype(jnp.int32))
+
+    def remote(src, dst, send, recv, dev):
+        return pltpu.make_async_remote_copy(
+            src_ref=src, dst_ref=dst, send_sem=send, recv_sem=recv,
+            device_id=dev, device_id_type=MESH,
+        )
+
+    def subs(body):
+        def step(sub, carry):
+            body(sub)
+            return carry
+
+        lax.fori_loop(0, SUBS, step, 0)
+
+    def piece(array, s, h, sub):
+        if array == 0:
+            m = hd // SUBS
+            return U.at[s, pl.ds(pl.multiple_of(h * hd + sub * m, m), m), :]
+        m = ff // SUBS
+        return Dn.at[s, h, pl.ds(pl.multiple_of(sub * m, m), m), :]
+
+    def to_pal(array, s, h, sub):
+        ref = piece(array, s, h, sub)
+        return remote(ref, ref, z_send.at[array, s, h, sub], z_recv.at[array, s, h, sub], {"fs": pal})
+
+    def to_inner(array, s, sub):
+        ref = piece(array, s, g, sub)
+        return remote(ref, ref, z_send.at[array, s, g, sub], z_recv.at[array, s, g, sub], {"fs": n - 1 - f})
+
+    def to_grp(array, s, h, sub):
+        ref = piece(array, s, h, sub)
+        return remote(ref, ref, y_send.at[array, s, sub], y_recv.at[array, s, sub], {"grp": other_g})
+
+    def t_copy():
+        r = pl.ds(pl.multiple_of(place * qr, qr), qr)
+        d = pl.ds(pl.multiple_of(rows + place * qr, qr), qr)
+        return remote(tok.at[r, :], tok.at[d, :], t_send, t_recv, {"fs": pal})
+
+    def g_copy(d):
+        r = pl.ds(pl.multiple_of(rows + place * qr, qr), qr)
+        return remote(tok.at[r, :], tok.at[r, :], g_send.at[d], g_recv.at[d], {"tp": peers[d]})
+
+    own_half = pl.ds(pl.multiple_of(core * hr, hr), hr)
+    mate_half = pl.ds(pl.multiple_of((1 - core) * hr, hr), hr)
+
+    def a_copy(q):
+        return remote(part.at[q, 1 - core], half_in.at[q], a_send.at[q], a_recv.at[q], {"tp": mate})
+
+    def b_copies(q):
+        away = pl.ds(pl.multiple_of(hr + (1 - chip) * qr, qr), qr)
+        return [
+            remote(pair.at[q, pl.ds(0, hr), :], pair_in.at[q, pl.ds(0, hr), :],
+                   b_send.at[0, q], b_recv.at[0, q], {"tp": across}),
+            remote(pair.at[q, away, :], pair_in.at[q, pl.ds(hr, qr), :],
+                   b_send.at[1, q], b_recv.at[1, q], {"tp": across}),
+        ]
+
+    def c_copy(q, r):
+        ref = summed.at[q, r, :]
+        return remote(ref, ref, c_send.at[q], c_recv.at[q], {"tp": mate})
+
+    def e_copy(q):
+        d = pl.ds(pl.multiple_of(place * qr, qr), qr)
+        return remote(quarter.at[q], half_in.at[q, d, :], e_send.at[q], e_recv.at[q], {"fs": pal})
+
+    def h_copy(q, d):
+        ref = half_in.at[q, pl.ds(pl.multiple_of(place * qr, qr), qr), :]
+        return remote(ref, ref, h_send.at[d, q], h_recv.at[d, q], {"tp": peers[d]})
+
+    sequence = [
+        (fi, g), (fi, other_g), (ri, g), (fo, g), (ri, other_g), (ro, g), (fo, other_g), (ro, other_g)
+    ]
+    sequence = [s * 2 + h for s, h in sequence]
+
+    def normed(read):
+        def norm(i, carry):
+            m = 16
+            r = pl.ds(pl.multiple_of(i * m, m), m)
+            total = jnp.concatenate([read(q, r) for q in range(blocks)], axis=-1)
+            out_ref[r, :] = layer_normed(tok[r, :], total, gain_ref[...], shift_ref[...])
+            return carry
+
+        lax.fori_loop(0, rows // 16, norm, 0)
+
+    @pl.when(jnp.logical_not(inner))
+    def _():
+        local[0].wait()
+        subs(lambda sub: to_pal(0, f, g, sub).start())
+        local[1].wait()
+        t_copy().start()
+        local[2].wait()
+        subs(lambda sub: to_pal(0, f, other_g, sub).start())
+        local[3].wait()
+        subs(lambda sub: to_pal(1, f, g, sub).start())
+        local[4].wait()
+        subs(lambda sub: to_pal(1, f, other_g, sub).start())
+        for q in sequence:
+            e_copy(q).wait_recv()
+            for d in range(3):
+                h_copy(q, d).start()
+        for q in sequence:
+            for d in range(3):
+                h_copy(q, d).wait_recv()
+        normed(lambda q, r: half_in[q, r, :].astype(jnp.float32))
+
+        def drain(sub):
+            for array in range(2):
+                to_pal(array, f, g, sub).wait_send()
+                to_pal(array, f, other_g, sub).wait_send()
+
+        subs(drain)
+        t_copy().wait_send()
+        for q in range(blocks):
+            for d in range(3):
+                h_copy(q, d).wait_send()
+
+    @pl.when(inner)
+    def _():
+        def up_dot(s, h, first=False):
+            r = pl.ds(pl.multiple_of(h * hd, hd), hd)
+            kc = pl.ds(pl.multiple_of(s * depth + h * hd, hd), hd)
+            tile = ff // 4
+
+            def body(j, carry):
+                js = pl.ds(pl.multiple_of(j * tile, tile), tile)
+                got = jnp.dot(tok[pl.ds(0, rows), kc], U[s, r, js], preferred_element_type=jnp.float32)
+                if first:
+                    acc[:, js] = got
+                else:
+                    acc[:, js] += got
+                return carry
+
+            lax.fori_loop(0, 4, body, 0)
+
+        def activated(x):
+            return jnp.square(jnp.maximum(x, 0.0)).astype(jnp.bfloat16)
+
+        def activate(i, carry):
+            m = rows // 12
+            r = pl.ds(pl.multiple_of(i * m, m), m)
+            hid[r, :] = activated(acc[r, :])
+            return carry
+
+        def outer_up(i, carry):
+            tile = ff // 4
+            r = pl.ds(pl.multiple_of(rows + (i // 4) * hr, hr), hr)
+            js = pl.ds(pl.multiple_of(lax.rem(i, 4) * tile, tile), tile)
+            got = jnp.dot(tok[r, pl.ds(0, depth)], U[0, :, js], preferred_element_type=jnp.float32)
+            for s in range(1, n):
+                got += jnp.dot(
+                    tok[r, pl.ds(s * depth, depth)], U[s, :, js], preferred_element_type=jnp.float32
+                )
+            hid[r, js] = activated(got)
+            return carry
+
+        def down_dot(q):
+            s, h = q // 2, lax.rem(q, 2)
+
+            def body(i, carry):
+                r = pl.ds(pl.multiple_of(i * hr, hr), hr)
+                d = pl.ds(pl.multiple_of((i // 2) * hr, hr), hr)
+                part[q, lax.rem(i, 2), d, :] = jnp.dot(
+                    hid[r, :], Dn[s, h], preferred_element_type=jnp.float32
+                ).astype(jnp.bfloat16)
+                return carry
+
+            lax.fori_loop(0, 4, body, 0)
+            a_copy(q).start()
+
+        def chip_sum(q):
+            a_copy(q).wait_recv()
+            pair[q] = (
+                part[q, core].astype(jnp.float32) + half_in[q].astype(jnp.float32)
+            ).astype(jnp.bfloat16)
+            for c in b_copies(q):
+                c.start()
+
+        def full_sum(q):
+            for c in b_copies(q):
+                c.wait_recv()
+            keep = pl.ds(pl.multiple_of(hr + chip * qr, qr), qr)
+            summed[q, own_half, :] = (
+                pair[q, pl.ds(0, hr), :].astype(jnp.float32) + pair_in[q, pl.ds(0, hr), :].astype(jnp.float32)
+            )
+            c_copy(q, own_half).start()
+            quarter[q] = (
+                pair[q, keep, :].astype(jnp.float32) + pair_in[q, pl.ds(hr, qr), :].astype(jnp.float32)
+            ).astype(jnp.bfloat16)
+            e_copy(q).start()
+
+        def take_r(array, s):
+            def body(sub):
+                to_inner(array, s, sub).wait_recv()
+                to_grp(array, s, g, sub).start()
+
+            subs(body)
+
+        def take_l(array, h, on):
+            def body(sub):
+                to_pal(array, fo, h, sub).wait_recv()
+                if on:
+                    to_inner(array, fo, sub).start()
+
+            subs(body)
+
+        def take_y(array, s):
+            subs(lambda sub: to_grp(array, s, other_g, sub).wait_recv())
+
+        local[0].wait()
+        subs(lambda sub: to_inner(0, f, sub).start())
+        for c in local[1:]:
+            c.wait()
+        up_dot(fi, 0, first=True)
+        up_dot(fi, 1)
+
+        def both(sub):
+            to_pal(0, fo, g, sub).wait_recv()
+            to_inner(0, fo, sub).start()
+            to_inner(0, ri, sub).wait_recv()
+            to_grp(0, ri, g, sub).start()
+
+        subs(both)
+        subs(lambda sub: to_inner(1, f, sub).start())
+        up_dot(fo, g)
+        up_dot(ri, g)
+        t_copy().wait_recv()
+        for d in range(3):
+            g_copy(d).start()
+        take_r(0, ro)
+        up_dot(ro, g)
+        take_y(0, ri)
+        up_dot(ri, other_g)
+        take_l(0, other_g, False)
+        up_dot(fo, other_g)
+        take_r(1, ri)
+        take_y(0, ro)
+        up_dot(ro, other_g)
+        lax.fori_loop(0, 12, activate, 0)
+        for d in range(3):
+            g_copy(d).wait_recv()
+        lax.fori_loop(0, 8, outer_up, 0)
+
+        needs = {
+            3: lambda: take_l(1, g, True),
+            4: lambda: take_y(1, ri),
+            5: lambda: take_r(1, ro),
+            6: lambda: take_l(1, other_g, False),
+            7: lambda: take_y(1, ro),
+        }
+        for i, q in enumerate(sequence):
+            if i in needs:
+                needs[i]()
+            down_dot(q)
+            if i > 0:
+                chip_sum(sequence[i - 1])
+            if i > 1:
+                full_sum(sequence[i - 2])
+        chip_sum(sequence[-1])
+        full_sum(sequence[-2])
+        full_sum(sequence[-1])
+        for q in range(blocks):
+            c_copy(q, mate_half).wait_recv()
+        normed(lambda q, r: summed[q, r, :])
+
+        def drain(sub):
+            for array in range(2):
+                to_inner(array, f, sub).wait_send()
+                to_inner(array, fo, sub).wait_send()
+                to_grp(array, ri, g, sub).wait_send()
+                to_grp(array, ro, g, sub).wait_send()
+
+        subs(drain)
+        for d in range(3):
+            g_copy(d).wait_send()
+        for q in range(blocks):
+            a_copy(q).wait_send()
+            for c in b_copies(q):
+                c.wait_send()
+            c_copy(q, own_half).wait_send()
+            e_copy(q).wait_send()
+
+
+def direct(n, tokens, up_weight, down_weight, norm_gain, norm_shift):
+    rows, width = tokens.shape
+    depth, ff = up_weight.shape
+    hw = down_weight.shape[1] // 2
+    blocks = 2 * n
+    bf16, f32 = jnp.bfloat16, jnp.float32
+    dma = pltpu.SemaphoreType.DMA
+    anywhere = pl.BlockSpec(memory_space=pl.ANY)
+    vmem = pl.BlockSpec(memory_space=pltpu.VMEM)
+    return pl.pallas_call(
+        functools.partial(kernel, n),
+        out_shape=jax.ShapeDtypeStruct((rows, width), bf16),
+        in_specs=[anywhere, anywhere, anywhere, vmem, vmem],
+        out_specs=vmem,
+        scratch_shapes=[
+            pltpu.VMEM((2 * rows, width), bf16),
+            pltpu.VMEM((n, depth, ff), bf16),
+            pltpu.VMEM((n, 2, ff, hw), bf16),
+            pltpu.VMEM((rows, ff), f32),
+            pltpu.VMEM((2 * rows, ff), bf16),
+            pltpu.VMEM((blocks, 2, rows, hw), bf16),
+            pltpu.VMEM((blocks, rows, hw), bf16),
+            pltpu.VMEM((blocks, rows, hw), bf16),
+            pltpu.VMEM((blocks, 3 * rows // 4, hw), bf16),
+            pltpu.VMEM((blocks, rows, hw), f32),
+            pltpu.VMEM((blocks, rows // 4, hw), bf16),
+            dma((5,)),
+            dma((2, n, 2, SUBS)), dma((2, n, 2, SUBS)),
+            dma((2, n, SUBS)), dma((2, n, SUBS)),
+            dma, dma,
+            dma((3,)), dma((3,)),
+            dma((blocks,)), dma((blocks,)),
+            dma((2, blocks)), dma((2, blocks)),
+            dma((blocks,)), dma((blocks,)),
+            dma((blocks,)), dma((blocks,)),
+            dma((3, blocks)), dma((3, blocks)),
+        ],
+        compiler_params=pltpu.CompilerParams(
+            collective_id=0, has_side_effects=True, vmem_limit_bytes=67043328
+        ),
+    )(tokens, up_weight, down_weight, norm_gain[None, :], norm_shift[None, :])
+
+
 def solution(mesh):
     placed = (P(("grp", "fs"), None), P("fs", "tp"), P("tp", "fs"), P(), P())
+    n = mesh.shape["fs"]
+    fits = mesh.shape["grp"] == 2 and mesh.shape["tp"] == 4 and n == 4
     return jax.shard_map(
-        shards, mesh=mesh, in_specs=placed, out_specs=P(("grp", "fs"), None), check_vma=False
+        functools.partial(direct, n) if fits else general,
+        mesh=mesh, in_specs=placed, out_specs=P(("grp", "fs"), None), check_vma=False,
     )

time: 403 us -> 185 us (0.46)
  waiting for transfers between devices: 358 us -> 0 us
  Pallas kernels: 0 us -> 180 us
  matrix products: 22 us -> 0 us
  between operations: 13.2 us -> 0.01 us
  other arithmetic: 4.49 us -> 0 us
    all_gather x3 -> x0, waiting for transfers between devices: 321 us -> none  [the longest x1 153 us: shards(): lax.all_gather(up_weight, 'fs', axis=0, tiled=True)]
    pallas_call x0 -> x1, Pallas kernels: none -> 180 us  [direct(): pl.pallas_call(functools.partial(kernel, n), out_shape=jax.ShapeDtypeStru...]
    reduce_scatter x1 -> x0, waiting for transfers between devices: 35.8 us -> none  [shards(): lax.psum_scatter(jnp.dot(hidden, down_full, preferred_element_type=jnp.fl...]
    dot_general x2 -> x0, matrix products: 22 us -> none  [the longest x1 11.9 us: shards(): jnp.dot(hidden, down_full, preferred_element_type=jnp.float32)]
  transfers between devices with their start and end apart: 4 -> 0, of which waited for: 4 -> 0; matrix products, arithmetic and copies ran while one was open for 3% -> 0% of each run, Pallas kernels for 0% -> 0%
where the time goes in v2:
time: 185 us; the launch traced here: 184 us
  Pallas kernels  180 us (97%)
  local copies, waits for them, and re-layouts  3.97 us (2%)
    pallas_call x1, Pallas kernels, direct(): pl.pallas_call(functools.partial(kernel, n), out_shape=jax.ShapeDtypeStru...  180 us
    unnamed x1, local copies, waits for them, and re-layouts  3.97 us

profile of v2, /device:TPU:1, one launch (start us, length us, event | category | flops | bytes accessed | tf_op | source)
XLA Modules:
  0.0 184.4 jit_solution(6840638887766623306)
XLA Ops:
  0.0 180.4 %shard_map.55 = bf16[768,2048]{1,0:T(8,128)(2,1)} custom-call(bf16[768,2048]{1,0:T(8,128)(2,1)} %tok_hbm.1, bf16[512,2048]{1,0:T(8,128)(2,1)} %up_hbm.1, bf16[2048,512]{1,0:T(8,128)(2,1)} %down_hbm.1, f32[1,2048]{1,0:T(1,128)} %bitcast.2, f32[1,2048]{1,0:T(1,128)} %bitcast.3), custom_call_target="tpu_custom_call" | custom-call | tf_op jit(solution)/shard_map/pallas_call | solution.py:388
  180.4 4.0 %copy.7 = bf16[768,2048]{1,0:T(8,128)(2,1)} copy(bf16[768,2048]{1,0:T(8,128)(2,1)} %shard_map.55) | data formatting | bytes 6291456

commit v3 on v2

--- a/solution.py
+++ b/solution.py
@@ -46,9 +46,9 @@
     n,
     tok_hbm, up_hbm, down_hbm, gain_ref, shift_ref,
     out_ref,
-    tok, U, Dn, acc, hid, part, half_in, pair, pair_in, summed, quarter,
+    tok, U, Dn, acc, hid, part, half_in, pair, pair_in, summed,
     loc_sem, z_send, z_recv, y_send, y_recv, t_send, t_recv, g_send, g_recv,
-    a_send, a_recv, b_send, b_recv, c_send, c_recv, e_send, e_recv, h_send, h_recv,
+    a_send, a_recv, b_send, b_recv, c_send, c_recv, e_send, e_recv,
 ):
     g, f, t = lax.axis_index("grp"), lax.axis_index("fs"), lax.axis_index("tp")
     core, chip = lax.rem(t, 2), t // 2
@@ -142,26 +142,31 @@
     def a_copy(q):
         return remote(part.at[q, 1 - core], half_in.at[q], a_send.at[q], a_recv.at[q], {"tp": mate})
 
-    def b_copies(q):
-        away = pl.ds(pl.multiple_of(hr + (1 - chip) * qr, qr), qr)
-        return [
-            remote(pair.at[q, pl.ds(0, hr), :], pair_in.at[q, pl.ds(0, hr), :],
-                   b_send.at[0, q], b_recv.at[0, q], {"tp": across}),
-            remote(pair.at[q, away, :], pair_in.at[q, pl.ds(hr, qr), :],
-                   b_send.at[1, q], b_recv.at[1, q], {"tp": across}),
-        ]
+    def b_copy(q):
+        return remote(
+            pair.at[q, pl.ds(0, hr), :], pair_in.at[q], b_send.at[q], b_recv.at[q], {"tp": across}
+        )
 
     def c_copy(q, r):
         ref = summed.at[q, r, :]
         return remote(ref, ref, c_send.at[q], c_recv.at[q], {"tp": mate})
 
     def e_copy(q):
-        d = pl.ds(pl.multiple_of(place * qr, qr), qr)
-        return remote(quarter.at[q], half_in.at[q, d, :], e_send.at[q], e_recv.at[q], {"fs": pal})
-
-    def h_copy(q, d):
-        ref = half_in.at[q, pl.ds(pl.multiple_of(place * qr, qr), qr), :]
-        return remote(ref, ref, h_send.at[d, q], h_recv.at[d, q], {"tp": peers[d]})
+        return remote(
+            pair.at[q, pl.ds(hr, hr), :], pair.at[q, pl.ds(0, hr), :], e_send.at[q], e_recv.at[q], {"fs": pal}
+        )
+
+    def full_sum(q):
+        b_copy(q).wait_recv()
+        summed[q, own_half, :] = (
+            pair[q, pl.ds(0, hr), :].astype(jnp.float32) + pair_in[q].astype(jnp.float32)
+        )
+        c_copy(q, own_half).start()
+
+    def normed_sums():
+        for q in range(blocks):
+            c_copy(q, mate_half).wait_recv()
+        normed(lambda q, r: summed[q, r, :])
 
     sequence = [
         (fi, g), (fi, other_g), (ri, g), (fo, g), (ri, other_g), (ro, g), (fo, other_g), (ro, other_g)
@@ -170,45 +175,47 @@
 
     def normed(read):
         def norm(i, carry):
-            m = 16
+            m = 64
             r = pl.ds(pl.multiple_of(i * m, m), m)
             total = jnp.concatenate([read(q, r) for q in range(blocks)], axis=-1)
             out_ref[r, :] = layer_normed(tok[r, :], total, gain_ref[...], shift_ref[...])
             return carry
 
-        lax.fori_loop(0, rows // 16, norm, 0)
+        lax.fori_loop(0, rows // 64, norm, 0)
 
     @pl.when(jnp.logical_not(inner))
     def _():
+        local[1].wait()
+        t_copy().start()
         local[0].wait()
         subs(lambda sub: to_pal(0, f, g, sub).start())
-        local[1].wait()
-        t_copy().start()
         local[2].wait()
         subs(lambda sub: to_pal(0, f, other_g, sub).start())
         local[3].wait()
         subs(lambda sub: to_pal(1, f, g, sub).start())
         local[4].wait()
-        subs(lambda sub: to_pal(1, f, other_g, sub).start())
-        for q in sequence:
+        for sub in range(SUBS - 1):
+            to_pal(1, f, other_g, sub).start()
+        for i, q in enumerate(sequence):
             e_copy(q).wait_recv()
-            for d in range(3):
-                h_copy(q, d).start()
-        for q in sequence:
-            for d in range(3):
-                h_copy(q, d).wait_recv()
-        normed(lambda q, r: half_in[q, r, :].astype(jnp.float32))
+            b_copy(q).start()
+            if i > 0:
+                full_sum(sequence[i - 1])
+        full_sum(sequence[-1])
+        normed_sums()
 
         def drain(sub):
             for array in range(2):
                 to_pal(array, f, g, sub).wait_send()
-                to_pal(array, f, other_g, sub).wait_send()
+            to_pal(0, f, other_g, sub).wait_send()
 
         subs(drain)
+        for sub in range(SUBS - 1):
+            to_pal(1, f, other_g, sub).wait_send()
         t_copy().wait_send()
         for q in range(blocks):
-            for d in range(3):
-                h_copy(q, d).wait_send()
+            b_copy(q).wait_send()
+            c_copy(q, own_half).wait_send()
 
     @pl.when(inner)
     def _():
@@ -268,20 +275,7 @@
             pair[q] = (
                 part[q, core].astype(jnp.float32) + half_in[q].astype(jnp.float32)
             ).astype(jnp.bfloat16)
-            for c in b_copies(q):
-                c.start()
-
-        def full_sum(q):
-            for c in b_copies(q):
-                c.wait_recv()
-            keep = pl.ds(pl.multiple_of(hr + chip * qr, qr), qr)
-            summed[q, own_half, :] = (
-                pair[q, pl.ds(0, hr), :].astype(jnp.float32) + pair_in[q, pl.ds(0, hr), :].astype(jnp.float32)
-            )
-            c_copy(q, own_half).start()
-            quarter[q] = (
-                pair[q, keep, :].astype(jnp.float32) + pair_in[q, pl.ds(hr, qr), :].astype(jnp.float32)
-            ).astype(jnp.bfloat16)
+            b_copy(q).start()
             e_copy(q).start()
 
         def take_r(array, s):
@@ -309,19 +303,14 @@
         up_dot(fi, 0, first=True)
         up_dot(fi, 1)
 
-        def both(sub):
-            to_pal(0, fo, g, sub).wait_recv()
-            to_inner(0, fo, sub).start()
-            to_inner(0, ri, sub).wait_recv()
-            to_grp(0, ri, g, sub).start()
-
-        subs(both)
-        subs(lambda sub: to_inner(1, f, sub).start())
-        up_dot(fo, g)
-        up_dot(ri, g)
+        take_r(0, ri)
         t_copy().wait_recv()
         for d in range(3):
             g_copy(d).start()
+        up_dot(ri, g)
+        take_l(0, g, True)
+        subs(lambda sub: to_inner(1, f, sub).start())
+        up_dot(fo, g)
         take_r(0, ro)
         up_dot(ro, g)
         take_y(0, ri)
@@ -336,11 +325,16 @@
             g_copy(d).wait_recv()
         lax.fori_loop(0, 8, outer_up, 0)
 
+        def take_last():
+            for sub in range(SUBS - 1):
+                to_pal(1, fo, other_g, sub).wait_recv()
+            to_grp(1, fo, other_g, SUBS - 1).wait_recv()
+
         needs = {
-            3: lambda: take_l(1, g, True),
+            3: lambda: (take_l(1, g, True), to_grp(1, fo, g, SUBS - 1).start()),
             4: lambda: take_y(1, ri),
             5: lambda: take_r(1, ro),
-            6: lambda: take_l(1, other_g, False),
+            6: take_last,
             7: lambda: take_y(1, ro),
         }
         for i, q in enumerate(sequence):
@@ -354,9 +348,7 @@
         chip_sum(sequence[-1])
         full_sum(sequence[-2])
         full_sum(sequence[-1])
-        for q in range(blocks):
-            c_copy(q, mate_half).wait_recv()
-        normed(lambda q, r: summed[q, r, :])
+        normed_sums()
 
         def drain(sub):
             for array in range(2):
@@ -366,12 +358,12 @@
                 to_grp(array, ro, g, sub).wait_send()
 
         subs(drain)
+        to_grp(1, fo, g, SUBS - 1).wait_send()
         for d in range(3):
             g_copy(d).wait_send()
         for q in range(blocks):
             a_copy(q).wait_send()
-            for c in b_copies(q):
-                c.wait_send()
+            b_copy(q).wait_send()
             c_copy(q, own_half).wait_send()
             e_copy(q).wait_send()
 
@@ -399,19 +391,17 @@
             pltpu.VMEM((blocks, 2, rows, hw), bf16),
             pltpu.VMEM((blocks, rows, hw), bf16),
             pltpu.VMEM((blocks, rows, hw), bf16),
-            pltpu.VMEM((blocks, 3 * rows // 4, hw), bf16),
+            pltpu.VMEM((blocks, rows // 2, hw), bf16),
             pltpu.VMEM((blocks, rows, hw), f32),
-            pltpu.VMEM((blocks, rows // 4, hw), bf16),
             dma((5,)),
             dma((2, n, 2, SUBS)), dma((2, n, 2, SUBS)),
             dma((2, n, SUBS)), dma((2, n, SUBS)),
             dma, dma,
             dma((3,)), dma((3,)),
             dma((blocks,)), dma((blocks,)),
-            dma((2, blocks)), dma((2, blocks)),
             dma((blocks,)), dma((blocks,)),
             dma((blocks,)), dma((blocks,)),
-            dma((3, blocks)), dma((3, blocks)),
+            dma((blocks,)), dma((blocks,)),
         ],
         compiler_params=pltpu.CompilerParams(
             collective_id=0, has_side_effects=True, vmem_limit_bytes=67043328

time: 185 us -> 159 us (0.86)
  Pallas kernels: 180 us -> 155 us
    pallas_call x1, Pallas kernels: 180 us -> 155 us  [direct(): pl.pallas_call(functools.partial(kernel, n), out_shape=jax.ShapeDtypeStru...]
where the time goes in v3:
time: 159 us
  Pallas kernels  155 us (97%)
  local copies, waits for them, and re-layouts  3.97 us (2%)
    pallas_call x1, Pallas kernels, direct(): pl.pallas_call(functools.partial(kernel, n), out_shape=jax.ShapeDtypeStru...  155 us
    unnamed x1, local copies, waits for them, and re-layouts  3.97 us

profile of v3, /device:TPU:1, one launch (start us, length us, event | category | flops | bytes accessed | tf_op | source)
XLA Modules:
  0.0 158.9 jit_solution(134760912793824975)
XLA Ops:
  0.0 155.0 %shard_map.55 = bf16[768,2048]{1,0:T(8,128)(2,1)} custom-call(bf16[768,2048]{1,0:T(8,128)(2,1)} %tok_hbm.1, bf16[512,2048]{1,0:T(8,128)(2,1)} %up_hbm.1, bf16[2048,512]{1,0:T(8,128)(2,1)} %down_hbm.1, f32[1,2048]{1,0:T(1,128)} %bitcast.2, f32[1,2048]{1,0:T(1,128)} %bitcast.3), custom_call_target="tpu_custom_call" | custom-call | tf_op jit(solution)/shard_map/pallas_call | solution.py:380
  155.0 4.0 %copy.7 = bf16[768,2048]{1,0:T(8,128)(2,1)} copy(bf16[768,2048]{1,0:T(8,128)(2,1)} %shard_map.55) | data formatting | bytes 6291456
